TPU v7x, 512 devices: a whole 4x4x16 slice. The times are simulated.
512 devices in a mesh: ep: 32 (over z, core), tp: 16 (over y, x).
Axes of the slice: x: 4, y: 4, z: 16, core: 2. Of those that a mesh axis runs over, the one named last changes fastest.
Arguments:
- queries: bfloat16 [8192, 2048], P('ep', 'tp'), may hold values from -6 to 6
- keys: bfloat16 [8192, 2048], P('ep', 'tp'), may hold values from -6 to 6
- values: bfloat16 [8192, 2048], P('ep', 'tp'), may hold values from -6 to 6
- gates: bfloat16 [8192, 2048], P('ep', 'tp'), may hold values from -6 to 6
- log_decay: float32 [8192, 16], P('ep', 'tp'), may hold values from -2 to 0
- out_weight: bfloat16 [2048, 2048], P(None, 'tp'), may hold values from -0.125 to 0.125
- moe_rows: bfloat16 [8192, 2048], P('ep'), may hold values from -140 to 140
- moe_gain: bfloat16 [2048], replicated, may hold values from 0.099609375 to 1.8984375
- routes: int32 [8192, 2], P('ep'), may hold values from 0 to 31, as said below
- route_weights: float32 [8192, 2], P('ep'), may hold values from 0.1 to 1
- gate_proj: bfloat16 [32, 2048, 4096], P('ep', None, 'tp'), may hold values from -0.125 to 0.125
- up_proj: bfloat16 [32, 2048, 4096], P('ep', None, 'tp'), may hold values from -0.125 to 0.125
- down_proj: bfloat16 [32, 4096, 2048], P('ep', None, 'tp'), may hold values from -0.09375 to 0.09375
Outputs:
- mixer_out: bfloat16 [8192, 2048], P('ep', 'tp')
- moe_out: bfloat16 [8192, 2048], P('ep', 'tp')
Inputs may be any that keep to these rules, and one draw needn't show every extreme that they name: `routes`: each row names two different experts of one group of 8 consecutive experts; in each aligned block of 256 rows every expert is named by exactly 16 rows.
All inputs are finite; a program needn't handle non-finite values.
Results may differ from a plain program's by a relative error of at most 0.011.
Values may be sent and summed in bfloat16 or wider, within the bound.
No kernel may reach another device: no remote copies, remote signals or barrier semaphores. Data moves between devices by JAX's collectives and lax.ppermute only.
A program may use at most 64 MiB of HBM per device.

v0:
```python
import jax
import jax.numpy as jnp
from jax import lax
from jax.sharding import Mesh
from jax.sharding import PartitionSpec as P

BLOCK = 128
EP = ("ep_0", "ep_1")
TP = ("tp_0", "tp_1")


def filled_with(array, identity):
    return jax.tree.map(
        lambda part, zero: jnp.zeros_like(part) + jnp.asarray(zero, part.dtype), array, identity
    )


def collected_together(array, axis):
    leaves = jax.tree.leaves(array)
    turns = sorted(range(len(leaves)), key=lambda k: -leaves[k].size)
    width = (1, *leaves[turns[0]].shape)[-1]
    lines = [
        jnp.pad(leaves[k].reshape(-1), (0, -leaves[k].size % width)).reshape(-1, width)
        for k in turns
    ]
    both, at, found = (lax.all_gather(jnp.concatenate(lines), axis), 0, {})
    for k, line in zip(turns, lines):
        piece = both[:, at : at + len(line)].reshape(len(both), -1)
        found[k] = piece[:, : leaves[k].size].reshape(-1, *leaves[k].shape)
        at += len(line)
    numbers = iter(range(len(leaves)))
    return jax.tree.map(lambda _: found[next(numbers)], array)


def carried_in(array, axes, combine, identity):
    before = start = filled_with(array, identity)
    total = array
    for axis in reversed(axes):
        peers, mine = (lax.axis_size(axis), lax.axis_index(axis))
        pieces = collected_together(total, axis)
        inside, total = (start, start)
        for k in range(peers):
            passed = k < mine
            total = combine(total, jax.tree.map(lambda part: part[k], pieces))
            inside = jax.tree.map(lambda new, old: jnp.where(passed, new, old), total, inside)
        before = combine(inside, before)
    return before


def whole_of(array, axes, dim):
    for axis in reversed(axes):
        array = lax.all_gather(array, axis, axis=dim, tiled=True)
    return array


def in_order(parts, dim):
    lengths = list(parts.shape[1:])
    lengths[dim] *= parts.shape[0]
    return jnp.moveaxis(parts, 0, dim).reshape(lengths)


def copy_for_each(array, axis):
    peers = lax.axis_size(axis)
    return lax.all_to_all(
        jnp.broadcast_to(array[None], (peers, *array.shape)), axis, 0, 0, tiled=True
    )


def collect(array, axis, dim):
    return in_order(copy_for_each(array, axis), dim)


def rotate(source, positions, heads_here, factor):
    row_count, feat_width = source.shape
    head_dim = feat_width // heads_here
    half_dim = head_dim // 2
    values_f = source.astype(jnp.float32).reshape(row_count, heads_here, head_dim)
    inverse = 10000.0 ** (-jnp.arange(half_dim, dtype=jnp.float32) / half_dim)
    angles = positions[:, None] * inverse[None, :]
    cosine = jnp.cos(angles)[:, None, :]
    sine_part = jnp.sin(angles)[:, None, :]
    first_half = values_f[..., :half_dim]
    second_half = values_f[..., half_dim:]
    turned = jnp.concatenate(
        [
            first_half * cosine - second_half * sine_part,
            first_half * sine_part + second_half * cosine,
        ],
        axis=-1,
    )
    return (turned * factor).astype(jnp.bfloat16).reshape(row_count, feat_width)


def chain_states(earlier, later):
    return (earlier[0] * later[0], later[0][:, None, None] * earlier[1] + later[1])


def retention_half(queries, keys, values, gates, log_decay, out_weight):
    row_count, feat_width = queries.shape
    heads_here = log_decay.shape[1]
    head_dim = feat_width // heads_here
    block_count = row_count // BLOCK
    positions = (lax.axis_index(EP) * row_count + jnp.arange(row_count, dtype=jnp.int32)).astype(
        jnp.float32
    )
    rot_q = rotate(queries, positions, heads_here, 1.0)
    rot_k = rotate(keys, positions, heads_here, head_dim ** (-0.5))
    block_shape = (block_count, BLOCK, heads_here, head_dim)
    q_blocks = rot_q.reshape(block_shape)
    k_blocks = rot_k.reshape(block_shape)
    v_blocks = values.reshape(block_shape)
    cumulative = jnp.cumsum(log_decay.reshape(block_count, BLOCK, heads_here), axis=1)
    across = jnp.swapaxes(cumulative, 1, 2)
    spread = across[..., :, None] - across[..., None, :]
    causal = jnp.arange(BLOCK)[:, None] >= jnp.arange(BLOCK)[None, :]
    weights = jnp.where(causal, jnp.exp(jnp.where(causal, spread, 0.0)), 0.0)
    scores = jnp.einsum("nihd,njhd->nhij", q_blocks, k_blocks, preferred_element_type=jnp.float32)
    rounded = (scores * weights).astype(jnp.bfloat16)
    inside = jnp.einsum("nhij,njhd->nihd", rounded, v_blocks, preferred_element_type=jnp.float32)
    ending = cumulative[:, -1, :]
    k_scaled = k_blocks.astype(jnp.float32) * jnp.exp(ending[:, None, :] - cumulative)[..., None]
    updates = jnp.einsum(
        "njhd,njhe->nhde", k_scaled, v_blocks.astype(jnp.float32), precision=lax.Precision.HIGHEST
    )

    def advance(carry_state, member):
        return (jnp.exp(member[0])[:, None, None] * carry_state + member[1], carry_state)

    zero_state = jnp.zeros((heads_here, head_dim, head_dim), jnp.float32)
    local_end, before = lax.scan(advance, zero_state, (ending, updates))
    device_decay = jnp.exp(jnp.sum(ending, axis=0))
    incoming = carried_in(
        (device_decay, local_end), EP, chain_states, (jnp.ones_like(device_decay), zero_state)
    )
    leading = jnp.cumsum(ending, axis=0) - ending
    entering = before + jnp.exp(leading)[:, :, None, None] * incoming[1][None]
    carried = (
        jnp.einsum(
            "nihd,nhde->nihe",
            q_blocks.astype(jnp.float32),
            entering,
            precision=lax.Precision.HIGHEST,
        )
        * jnp.exp(cumulative)[..., None]
    )
    retained = (inside + carried).reshape(row_count, heads_here, head_dim)
    gate_f = gates.astype(jnp.float32).reshape(row_count, heads_here, head_dim)
    scaled = retained * lax.rsqrt(jnp.mean(retained * retained, axis=-1, keepdims=True) + 1e-05)
    head_out = (scaled * jax.nn.silu(gate_f)).astype(jnp.bfloat16).reshape(row_count, feat_width)
    projected = jnp.dot(whole_of(head_out, TP, 1), out_weight, preferred_element_type=jnp.float32)
    return projected.astype(jnp.bfloat16)


def expert_half(moe_rows, moe_gain, routes, route_weights, gate_proj, up_proj, down_proj):
    row_count, feat_width = moe_rows.shape
    experts = lax.axis_size(EP)
    capacity = 2 * row_count // experts
    as_float = moe_rows.astype(jnp.float32)
    normed = (
        as_float
        * lax.rsqrt(jnp.mean(as_float * as_float, axis=-1, keepdims=True) + 1e-06)
        * moe_gain.astype(jnp.float32)
    ).astype(jnp.bfloat16)
    flat_ids = routes.reshape(-1)
    onehot = (flat_ids[:, None] == jnp.arange(experts, dtype=jnp.int32)[None, :]).astype(jnp.int32)
    slot_rank = jnp.sum((jnp.cumsum(onehot, axis=0) - onehot) * onehot, axis=1)
    target = flat_ids * capacity + slot_rank
    source_row = (
        jnp.zeros((experts * capacity,), jnp.int32)
        .at[target]
        .set(jnp.arange(2 * row_count, dtype=jnp.int32) // 2)
    )
    outgoing = normed[source_row].reshape(experts, capacity, feat_width)
    w_gate = gate_proj[0]
    w_up = up_proj[0]
    w_down = down_proj[0]
    share_size = capacity // lax.axis_size(TP)
    own_share = lax.dynamic_slice_in_dim(outgoing, lax.axis_index(TP) * share_size, share_size, 1)
    arrived_share = lax.all_to_all(own_share, EP, split_axis=0, concat_axis=0, tiled=True)
    arrived = collect(arrived_share, TP, 1)
    gate_part = jnp.einsum("scd,df->scf", arrived, w_gate, preferred_element_type=jnp.float32)
    up_part = jnp.einsum("scd,df->scf", arrived, w_up, preferred_element_type=jnp.float32)
    hidden = (jax.nn.silu(gate_part) * up_part).astype(jnp.bfloat16)
    expert_out = jnp.einsum(
        "scf,fd->scd",
        lax.all_gather(hidden, TP, axis=2, tiled=True),
        w_down,
        preferred_element_type=jnp.float32,
    ).astype(jnp.bfloat16)
    returned = lax.all_to_all(expert_out, EP, split_axis=0, concat_axis=0, tiled=True)
    picked = returned.reshape(experts * capacity, -1)[target].reshape(row_count, 2, -1)
    return jnp.sum(picked.astype(jnp.float32) * route_weights[:, :, None], axis=1).astype(
        jnp.bfloat16
    )


def on_device(
    queries,
    keys,
    values,
    gates,
    log_decay,
    out_weight,
    moe_rows,
    moe_gain,
    routes,
    route_weights,
    gate_proj,
    up_proj,
    down_proj,
):
    mixer_out = retention_half(queries, keys, values, gates, log_decay, out_weight)
    moe_out = expert_half(moe_rows, moe_gain, routes, route_weights, gate_proj, up_proj, down_proj)
    return (mixer_out, moe_out)


def solution(mesh):
    torus = Mesh(mesh.devices.reshape(16, 2, 4, 4), ("ep_0", "ep_1", "tp_0", "tp_1"))
    return jax.shard_map(
        on_device,
        mesh=torus,
        in_specs=(
            P(EP, TP),
            P(EP, TP),
            P(EP, TP),
            P(EP, TP),
            P(EP, TP),
            P(None, TP),
            P(EP, None),
            P(),
            P(EP, None),
            P(EP, None),
            P(EP, None, TP),
            P(EP, None, TP),
            P(EP, None, TP),
        ),
        out_specs=(P(EP, TP), P(EP, TP)),
        check_vma=False,
    )
```

profile of v0, /device:TPU:2, one launch (start us, length us, event | category | flops | bytes accessed | tf_op | source)
XLA Modules:
  0.0 250.1 jit_solution(12538296000440214369)
XLA Ops:
  7.2 1.0 copy.44
  8.4 0.7 broadcast_multiply_fusion
  9.1 1.2 reduce-window.18
  11.0 2.4 scatter_custom_fusion
  13.5 0.7 convert_element_type.89
  14.2 1.5 fusion
  16.0 3.3 %gather_fusion = bf16[512,2048]{1,0:T(8,128)(2,1)} fusion(bf16[256,2048]{1,0:T(8,128)(2,1)S(1)} %fusion.2, s32[1024]{0:T(1024)S(1)} %pad_clamp_fusion.1), kind=kCustom, calls=%fused_computation | custom fusion | bytes 4196352 | tf_op jit(solution)/shard_map/gather | solution.py:173
  19.4 1.5 constant_dynamic-slice_fusion.1
  20.9 0.5 broadcast.370
  21.4 1.4 reduce.10
  22.8 0.7 reshape.656
  23.5 15.5 %all-to-all-start = ((bf16[32,2,1024]{2,1,0:T(2,128)(2,1)}), bf16[32,2,1024]{2,1,0:T(2,128)(2,1)S(1)}, u32[]{:S(2)}, u32[]{:S(2)}) async-start(bf16[32,2,1024]{2,1,0:T(2,128)(2,1)} %reshape.656), calls=%async_computation | async-start | bytes 262144 | tf_op jit(solution)/shard_map/all_to_all | solution.py:179
  39.4 0.6 slice_reduce_fusion.1
  40.2 0.6 fusion.34
  40.9 0.6 fusion.80
  41.9 2.4 while.13
  41.9 0.6 fusion.88
  42.5 0.6 bitcast_add_fusion.2
  43.1 0.6 fusion.88
  43.7 0.6 bitcast_add_fusion.2
  44.9 0.5 pad_bitcast_fusion.1
  45.5 10.7 %all-to-all-done = bf16[32,2,1024]{2,1,0:T(2,128)(2,1)S(1)} async-done(((bf16[32,2,1024]{2,1,0:T(2,128)(2,1)}), bf16[32,2,1024]{2,1,0:T(2,128)(2,1)S(1)}, u32[]{:S(2)}, u32[]{:S(2)}) %all-to-all-start) | async-done | bytes 131104 | tf_op jit(solution)/shard_map/all_to_all | solution.py:179
  56.4 1.6 broadcast_in_dim.33
  58.0 7.5 %all-to-all-start.1 = ((bf16[16,32,1,2048]{3,1,2,0:T(8,128)(2,1)}), bf16[16,32,1,2048]{3,1,2,0:T(8,128)(2,1)S(1)}, u32[]{:S(2)}, u32[]{:S(2)}) async-start(bf16[16,32,1,2048]{3,1,2,0:T(8,128)(2,1)} %broadcast_in_dim.33), calls=%async_computation.1 | async-start | bytes 4194304 | tf_op jit(solution)/shard_map/all_to_all | solution.py:64
  65.6 1.9 all-gather.2
  67.5 0.6 fusion.79
  70.0 0.7 fusion.66
  70.6 0.6 maximum_bitcast_fusion.1
  71.3 20.4 %all-to-all-done.1 = bf16[16,32,1,2048]{3,1,2,0:T(8,128)(2,1)S(1)} async-done(((bf16[16,32,1,2048]{3,1,2,0:T(8,128)(2,1)}), bf16[16,32,1,2048]{3,1,2,0:T(8,128)(2,1)S(1)}, u32[]{:S(2)}, u32[]{:S(2)}) %all-to-all-start.1) | async-done | bytes 2097184 | tf_op jit(solution)/shard_map/all_to_all | solution.py:64
  91.7 0.7 fusion.5
  92.5 0.5 copy-done.12
  92.9 1.4 fusion.10
  94.5 0.9 reduce-window.14
  96.0 0.6 fusion.72
  96.6 36.7 %all-gather.12.cloned.1.call-done = f32[16,129,128]{2,1,0:T(8,128)} async-done(((f32[1,129,128]{2,1,0:T(8,128)}), f32[16,129,128]{2,1,0:T(8,128)}) %all-gather.12.cloned.1.call-update) | async-done | bytes 1056784 | tf_op jit(solution)/shard_map/all_gather | solution.py:26
  133.3 0.8 slice.250
  134.2 0.6 fusion.78
  135.4 11.5 %fusion.57 = f32[128,128]{1,0:T(8,128)S(1)} fusion(f32[16,129,128]{2,1,0:T(8,128)} %all-gather.12.cloned.1.call-done, f32[2,129,128]{2,1,0:T(8,128)S(1)} %all-gather.2, f32[]{:T(128)} %bitcast.46, f32[]{:T(128)} %bitcast.45, f32[]{:T(128)} %bitcast.44, f32[]{:T(128)} %bitcast.43, f32[]{:T(128)} %bitcast.42, f32[]{:T(128)} %bitcast.41, f32[]{:T(128)} %bitcast.40, ...), kind=kLoop, calls=%fused_computation.81 | loop fusion | flops 884736 | bytes 1245278 | tf_op jit(solution)/shard_map/mul | solution.py:136
  146.9 1.2 fusion.14
  148.7 13.4 %all_gather.25 = bf16[256,512]{1,0:T(8,128)(2,1)} all-gather(bf16[256,128]{1,0:T(8,128)(2,1)S(1)} %fusion.50), channel_id=1, replica_groups=mesh['ep_0'=16,'ep_1'=2,'tp_0'=4,'tp_1'=4] {'tp_1'}, dimensions={1}, use_global_device_ids=true | all-gather | bytes 327680 | tf_op jit(solution)/shard_map/all_gather | solution.py:52
  162.2 43.0 %all-gather.10.cloned.1.call-done = bf16[32,16,4096]{2,0,1:T(8,128)(2,1)} async-done(((bf16[32,16,256]{2,0,1:T(8,128)(2,1)}), bf16[32,16,4096]{2,0,1:T(8,128)(2,1)}) %all-gather.10.cloned.1.call-update) | async-done | bytes 4194320 | tf_op jit(solution)/shard_map/all_gather | solution.py:186
  205.2 3.4 %fusion.16 = bf16[32,16,128]{2,0,1:T(8,128)(2,1)S(1)} fusion(bf16[32,16,4096]{2,0,1:T(8,128)(2,1)} %all-gather.10.cloned.1.call-done, bf16[1,4096,128]{2,1,0:T(8,128)(2,1)S(1)} %copy-done.13), kind=kOutput, calls=%fused_computation.25 | convolution fusion | flops 536870912 | bytes 5373952 | tf_op jit(solution)/shard_map/scf,fd->scd/dot_general | solution.py:184
  208.6 0.7 copy.58
  209.3 12.6 %all-to-all-start.2 = ((bf16[32,16,128]{2,1,0:T(8,128)(2,1)}), bf16[32,16,128]{2,1,0:T(8,128)(2,1)S(1)}, u32[]{:S(2)}, u32[]{:S(2)}) async-start(bf16[32,16,128]{2,1,0:T(8,128)(2,1)} %copy.58), calls=%async_computation.2 | async-start | bytes 262144 | tf_op jit(solution)/shard_map/all_to_all | solution.py:190
  222.1 16.8 %all-gather.8.cloned.1.call-done = bf16[256,2048]{1,0:T(8,128)(2,1)} async-done(((bf16[256,512]{1,0:T(8,128)(2,1)}), bf16[256,2048]{1,0:T(8,128)(2,1)}) %all-gather.8.cloned.1.call-update) | async-done | bytes 1048592 | tf_op jit(solution)/shard_map/all_gather | solution.py:52
  238.9 2.3 convolution_convert_fusion
  241.2 1.3 gather_fusion.1
  242.5 1.1 fusion.20
  (72 shorter events, 3.4 us)
Async XLA Ops:
  7.2 84.6 %copy-start = (bf16[1,2048,256]{2,1,0:T(8,128)(2,1)S(1)}, bf16[1,2048,256]{2,1,0:T(8,128)(2,1)}, u32[]{:S(2)}) copy-start(bf16[1,2048,256]{2,1,0:T(8,128)(2,1)} %param.25) | copy-start | bytes 3145732
  7.2 8.5 %copy-start.1 = (bf16[256,2048]{1,0:T(8,128)(2,1)S(1)}, bf16[256,2048]{1,0:T(8,128)(2,1)}, u32[]{:S(2)}) copy-start(bf16[256,2048]{1,0:T(8,128)(2,1)} %param.21) | copy-start | bytes 3145732
  16.0 23.1 %copy-start.10 = (f32[256,1]{0,1:T(1,128)S(1)}, f32[256,1]{0,1:T(1,128)}, u32[]{:S(2)}) copy-start(f32[256,1]{0,1:T(1,128)} %param.19) | copy-start | bytes 3076
  16.0 24.1 %copy-start.4 = (bf16[256,128]{1,0:T(8,128)(2,1)S(1)}, bf16[256,128]{1,0:T(8,128)(2,1)}, u32[]{:S(2)}) copy-start(bf16[256,128]{1,0:T(8,128)(2,1)} %param.16) | copy-start | bytes 196612
  16.0 24.1 %copy-start.5 = (bf16[256,128]{1,0:T(8,128)(2,1)S(1)}, bf16[256,128]{1,0:T(8,128)(2,1)}, u32[]{:S(2)}) copy-start(bf16[256,128]{1,0:T(8,128)(2,1)} %param.15) | copy-start | bytes 196612
  19.4 22.1 %copy-start.6 = (bf16[256,128]{1,0:T(8,128)(2,1)S(1)}, bf16[256,128]{1,0:T(8,128)(2,1)}, u32[]{:S(2)}) copy-start(bf16[256,128]{1,0:T(8,128)(2,1)} %param.17) | copy-start | bytes 196612
  23.5 32.7 %all-to-all-start = ((bf16[32,2,1024]{2,1,0:T(2,128)(2,1)}), bf16[32,2,1024]{2,1,0:T(2,128)(2,1)S(1)}, u32[]{:S(2)}, u32[]{:S(2)}) async-start(bf16[32,2,1024]{2,1,0:T(2,128)(2,1)} %reshape.656), calls=%async_computation | async-start | bytes 262144 | tf_op jit(solution)/shard_map/all_to_all | solution.py:179
  44.3 1.2 copy-start.3
  44.3 13.7 %copy-start.9 = (f32[2,1]{0,1:T(1,128)}, f32[2,1]{0,1:T(1,128)S(1)}, u32[]{:S(2)}) copy-start(f32[2,1]{0,1:T(1,128)S(1)} %get-tuple-element.178) | copy-start | bytes 28
  58.0 7.5 %copy-start.11 = (f32[1,128]{1,0:T(1,128)S(1)}, f32[1,128]{1,0:T(1,128)}, u32[]{:S(2)}) copy-start(f32[1,128]{1,0:T(1,128)} %pad_bitcast_fusion.1) | copy-start | bytes 1540
  58.0 33.7 %all-to-all-start.1 = ((bf16[16,32,1,2048]{3,1,2,0:T(8,128)(2,1)}), bf16[16,32,1,2048]{3,1,2,0:T(8,128)(2,1)S(1)}, u32[]{:S(2)}, u32[]{:S(2)}) async-start(bf16[16,32,1,2048]{3,1,2,0:T(8,128)(2,1)} %broadcast_in_dim.33), calls=%async_computation.1 | async-start | bytes 4194304 | tf_op jit(solution)/shard_map/all_to_all | solution.py:64
  65.5 67.8 %all-gather.12.cloned.1.call-start = ((), (), s32[]{:S(2)}) async-start(), calls=%async_computation.5 | async-start | bytes 1183744 | tf_op jit(solution)/shard_map/all_gather | solution.py:26
  71.3 133.9 %all-gather.10.cloned.1.call-start = ((), (), s32[]{:S(2)}) async-start(), calls=%async_computation.4 | async-start | bytes 4456448 | tf_op jit(solution)/shard_map/all_gather | solution.py:186
  91.7 1.2 copy-start.12
  94.4 54.2 %copy-start.7 = (bf16[256,128]{1,0:T(8,128)(2,1)S(1)}, bf16[256,128]{1,0:T(8,128)(2,1)}, u32[]{:S(2)}) copy-start(bf16[256,128]{1,0:T(8,128)(2,1)} %param.18) | copy-start | bytes 196612
  94.4 110.8 %copy-start.13 = (bf16[1,4096,128]{2,1,0:T(8,128)(2,1)S(1)}, bf16[1,4096,128]{2,1,0:T(8,128)(2,1)}, u32[]{:S(2)}) copy-start(bf16[1,4096,128]{2,1,0:T(8,128)(2,1)} %param.27) | copy-start | bytes 3145732
  94.4 144.5 %all-gather.8.cloned.1.call-start = ((), (), s32[]{:S(2)}) async-start(), calls=%async_computation.3 | async-start | bytes 1310720 | tf_op jit(solution)/shard_map/all_gather | solution.py:52
  162.1 59.7 %copy-start.8 = (f32[256,2]{0,1:T(2,128)S(1)}, f32[256,2]{0,1:T(2,128)}, u32[]{:S(2)}) copy-start(f32[256,2]{0,1:T(2,128)} %param.24) | copy-start | bytes 6148
  162.2 76.7 %copy-start.2 = (bf16[2048,128]{1,0:T(8,128)(2,1)S(1)}, bf16[2048,128]{1,0:T(8,128)(2,1)}, u32[]{:S(2)}) copy-start(bf16[2048,128]{1,0:T(8,128)(2,1)} %param.20) | copy-start | bytes 1572868
  209.3 31.9 %all-to-all-start.2 = ((bf16[32,16,128]{2,1,0:T(8,128)(2,1)}), bf16[32,16,128]{2,1,0:T(8,128)(2,1)S(1)}, u32[]{:S(2)}, u32[]{:S(2)}) async-start(bf16[32,16,128]{2,1,0:T(8,128)(2,1)} %copy.58), calls=%async_computation.2 | async-start | bytes 262144 | tf_op jit(solution)/shard_map/all_to_all | solution.py:190
Sparse Core Ops, SparseCore 0:
  71.4 61.8 all-gather.11
  136.3 68.8 all-gather.9
  207.3 31.5 all-gather.7
where the time goes:
time: 251 us; the launch traced here: 250 us
  waiting for transfers between devices  128 us (51%)
  starting transfers between devices  35.6 us (14%)
  other arithmetic  24.8 us (10%)
  local copies, waits for them, and re-layouts  18.7 us (7%)
  between operations  18 us (7%)
  blocking collectives  15.3 us (6%)
  matrix products  9.84 us (4%)
    all_gather x1, waiting for transfers between devices, expert_half(): lax.all_gather(hidden, TP, axis=2, tiled=True)  43 us
    all_gather x1, waiting for transfers between devices, collected_together(): both, at, found = (lax.all_gather(jnp.concatenate(lines), axis), 0, {})  36.7 us
    all_to_all x1, waiting for transfers between devices, copy_for_each(): lax.all_to_all(jnp.broadcast_to(array[None], (peers, *array.shape)), axis...  20.4 us
    all_gather x1, waiting for transfers between devices, whole_of(): array = lax.all_gather(array, axis, axis=dim, tiled=True)  16.8 us
    all_to_all x1, starting transfers between devices, expert_half(): lax.all_to_all(own_share, EP, split_axis=0, concat_axis=0, tiled=True)  15.5 us
    all_gather x1, blocking collectives, whole_of(): array = lax.all_gather(array, axis, axis=dim, tiled=True)  13.4 us
    all_to_all x1, starting transfers between devices, expert_half(): lax.all_to_all(expert_out, EP, split_axis=0, concat_axis=0, tiled=True)  12.6 us
    mul x1, other arithmetic, retention_half(): entering = before + jnp.exp(leading)[:, :, None, None] * incoming[1][None]  11.5 us
  transfers between devices with their start and end apart: 6, of which 5 were waited for; matrix products, arithmetic and copies ran while one was open for 13% of the time, Pallas kernels for 0%

commit v1 on v0

--- a/solution.py
+++ b/solution.py
@@ -183,7 +183,7 @@
     hidden = (jax.nn.silu(gate_part) * up_part).astype(jnp.bfloat16)
     expert_out = jnp.einsum(
         "scf,fd->scd",
-        lax.all_gather(hidden, TP, axis=2, tiled=True),
+        jnp.concatenate(lax.all_to_all(jnp.stack([hidden] * lax.axis_size(TP)), TP, 0, 0), axis=2),
         w_down,
         preferred_element_type=jnp.float32,
     ).astype(jnp.bfloat16)

time: 251 us -> 213 us (0.85)
  waiting for transfers between devices: 128 us -> 76.7 us
  local copies, waits for them, and re-layouts: 18.7 us -> 24.8 us
  starting transfers between devices: 35.6 us -> 41.4 us
  blocking collectives: 15.3 us -> 19.3 us
  matrix products: 9.84 us -> 6.72 us
    all_gather x1 -> x0, waiting for transfers between devices: 43 us -> none  [expert_half(): lax.all_gather(hidden, TP, axis=2, tiled=True)]
    all_to_all x0 -> x1, starting transfers between devices: none -> 8.12 us  [expert_half(): lax.all_to_all(jnp.stack([hidden] * lax.axis_size(TP)), TP, 0, 0)]
    all_to_all x1, waiting for transfers between devices: 20.4 us -> 14.6 us  [copy_for_each(): lax.all_to_all(jnp.broadcast_to(array[None], (peers, *array.shape)), axis...]
    all_gather x1, blocking collectives: 13.4 us -> 17.4 us  [whole_of(): array = lax.all_gather(array, axis, axis=dim, tiled=True)]
    all_gather x1, waiting for transfers between devices: 16.8 us -> 13.8 us  [whole_of(): array = lax.all_gather(array, axis, axis=dim, tiled=True)]
    all_gather x1, waiting for transfers between devices: 36.7 us -> 33.9 us  [collected_together(): both, at, found = (lax.all_gather(jnp.concatenate(lines), axis), 0, {})]
    reshape x0 -> x1, local copies, waits for them, and re-layouts: none -> 2.82 us  [expert_half(): jnp.concatenate(lax.all_to_all(jnp.stack([hidden] * lax.axis_size(TP)), T...]
    all_to_all x1, waiting for transfers between devices: 10.7 us -> 13.4 us  [expert_half(): lax.all_to_all(own_share, EP, split_axis=0, concat_axis=0, tiled=True)]
  transfers between devices with their start and end apart: 6 -> 6, of which waited for: 5 -> 5; matrix products, arithmetic and copies ran while one was open for 13% -> 17% of each run, Pallas kernels for 0% -> 0%
where the time goes in v1:
time: 213 us; the launch traced here: 212 us
  waiting for transfers between devices  76.7 us (36%)
  starting transfers between devices  41.4 us (19%)
  other arithmetic  25.3 us (12%)
  local copies, waits for them, and re-layouts  24.8 us (12%)
  blocking collectives  19.3 us (9%)
  between operations  18.2 us (9%)
  matrix products  6.72 us (3%)
    all_gather x1, waiting for transfers between devices, collected_together(): both, at, found = (lax.all_gather(jnp.concatenate(lines), axis), 0, {})  33.9 us
    all_gather x1, blocking collectives, whole_of(): array = lax.all_gather(array, axis, axis=dim, tiled=True)  17.4 us
    all_to_all x1, starting transfers between devices, expert_half(): lax.all_to_all(own_share, EP, split_axis=0, concat_axis=0, tiled=True)  15.5 us
    all_to_all x1, waiting for transfers between devices, copy_for_each(): lax.all_to_all(jnp.broadcast_to(array[None], (peers, *array.shape)), axis...  14.6 us
    all_gather x1, waiting for transfers between devices, whole_of(): array = lax.all_gather(array, axis, axis=dim, tiled=True)  13.8 us
    all_to_all x1, waiting for transfers between devices, expert_half(): lax.all_to_all(own_share, EP, split_axis=0, concat_axis=0, tiled=True)  13.4 us
    mul x1, other arithmetic, retention_half(): entering = before + jnp.exp(leading)[:, :, None, None] * incoming[1][None]  11.4 us
    all_to_all x1, starting transfers between devices, expert_half(): lax.all_to_all(expert_out, EP, split_axis=0, concat_axis=0, tiled=True)  10.1 us
  transfers between devices with their start and end apart: 6, of which 5 were waited for; matrix products, arithmetic and copies ran while one was open for 17% of the time, Pallas kernels for 0%

profile of v1, /device:TPU:2, one launch (start us, length us, event | category | flops | bytes accessed | tf_op | source)
XLA Modules:
  0.0 212.4 jit_solution(13796839068858657062)
XLA Ops:
  7.2 1.0 copy.45
  8.4 0.7 broadcast_multiply_fusion
  9.1 1.2 reduce-window.18
  11.0 2.4 %scatter_custom_fusion = s32[512]{0:T(512)S(1)} fusion(s32[512]{0:T(512)S(1)} %bitcast.174, s32[512]{0:T(512)S(1)} %add_select_fusion, s32[]{:T(128)} %constant.60.clone.1), kind=kCustom, calls=%fused_computation.126 | custom fusion | bytes 2052 | tf_op jit(solution)/shard_map/scatter | solution.py:171
  13.5 0.7 convert_element_type.89
  14.2 1.5 fusion
  16.0 3.3 %gather_fusion = bf16[512,2048]{1,0:T(8,128)(2,1)} fusion(bf16[256,2048]{1,0:T(8,128)(2,1)S(1)} %fusion.2, s32[1024]{0:T(1024)S(1)} %pad_clamp_fusion.1), kind=kCustom, calls=%fused_computation | custom fusion | bytes 4196352 | tf_op jit(solution)/shard_map/gather | solution.py:173
  19.4 1.5 constant_dynamic-slice_fusion.1
  20.9 0.5 broadcast.372
  21.4 1.4 reduce.10
  22.8 0.7 reshape.666
  23.5 15.5 %all-to-all-start = ((bf16[32,2,1024]{2,1,0:T(2,128)(2,1)}), bf16[32,2,1024]{2,1,0:T(2,128)(2,1)S(1)}, u32[]{:S(2)}, u32[]{:S(2)}) async-start(bf16[32,2,1024]{2,1,0:T(2,128)(2,1)} %reshape.666), calls=%async_computation | async-start | bytes 262144 | tf_op jit(solution)/shard_map/all_to_all | solution.py:179
  39.3 0.6 slice_reduce_fusion.1
  40.7 0.6 pad_bitcast_fusion.1
  41.4 1.2 fusion.33
  42.7 13.4 %all-to-all-done = bf16[32,2,1024]{2,1,0:T(2,128)(2,1)S(1)} async-done(((bf16[32,2,1024]{2,1,0:T(2,128)(2,1)}), bf16[32,2,1024]{2,1,0:T(2,128)(2,1)S(1)}, u32[]{:S(2)}, u32[]{:S(2)}) %all-to-all-start) | async-done | bytes 131104 | tf_op jit(solution)/shard_map/all_to_all | solution.py:179
  56.4 1.6 broadcast_in_dim.33
  58.0 7.6 %all-to-all-start.1 = ((bf16[16,32,1,2048]{3,1,2,0:T(8,128)(2,1)}), bf16[16,32,1,2048]{3,1,2,0:T(8,128)(2,1)S(1)}, u32[]{:S(2)}, u32[]{:S(2)}) async-start(bf16[16,32,1,2048]{3,1,2,0:T(8,128)(2,1)} %broadcast_in_dim.33), calls=%async_computation.1 | async-start | bytes 4194304 | tf_op jit(solution)/shard_map/all_to_all | solution.py:64
  65.6 0.6 fusion.79
  66.6 5.2 %while.13 = (s32[]{:T(128)}, f32[1,128,128]{2,1,0:T(8,128)S(1)}, f32[2,1,128,128]{3,2,1,0:T(8,128)}, f32[2,1]{0,1:T(1,128)}, f32[2,1,128,128]{3,2,1,0:T(8,128)S(1)}, /*index=5*/s32[]{:T(128)}, s32[]{:T(128)}) while((s32[]{:T(128)}, f32[1,128,128]{2,1,0:T(8,128)S(1)}, f32[2,1,128,128]{3,2,1,0:T(8,128)}, f32[2,1]{0,1:T(1,128)}, ...), condition=%wide.region_2.3_spmd.clone, body=%wide.region_1.2_spmd.clone.sunk | while | flops 65539 | bytes 328300 | solution.py:130
  66.6 0.6 bitcast_dynamic-update-slice_fusion.2
  67.2 1.3 fusion.87
  68.5 0.6 bitcast_add_fusion.2
  69.2 0.6 bitcast_dynamic-update-slice_fusion.2
  69.8 1.3 fusion.87
  71.1 0.6 bitcast_add_fusion.2
  71.8 1.9 all-gather.2
  73.7 0.5 fusion.78
  76.0 0.6 fusion.65
  76.6 0.6 maximum_bitcast_fusion.1
  77.2 14.6 %all-to-all-done.1 = bf16[16,32,1,2048]{3,1,2,0:T(8,128)(2,1)S(1)} async-done(((bf16[16,32,1,2048]{3,1,2,0:T(8,128)(2,1)}), bf16[16,32,1,2048]{3,1,2,0:T(8,128)(2,1)S(1)}, u32[]{:S(2)}, u32[]{:S(2)}) %all-to-all-start.1) | async-done | bytes 2097184 | tf_op jit(solution)/shard_map/all_to_all | solution.py:64
  91.8 0.7 fusion.5
  93.0 0.7 fusion.10
  93.9 2.4 %stack.2 = bf16[16,32,16,256]{3,2,1,0:T(8,128)(2,1)} broadcast(bf16[32,16,256]{2,1,0:T(8,128)(2,1)S(1)} %copy.49), dimensions={1,2,3} | broadcast | bytes 4456448 | tf_op jit(solution)/shard_map/stack | solution.py:186
  96.3 8.1 %all-to-all-start.2 = ((bf16[16,32,16,256]{3,2,1,0:T(8,128)(2,1)}), bf16[16,32,16,256]{3,2,1,0:T(8,128)(2,1)}, u32[]{:S(2)}, u32[]{:S(2)}) async-start(bf16[16,32,16,256]{3,2,1,0:T(8,128)(2,1)} %stack.2), calls=%async_computation.2 | async-start | bytes 8388608 | tf_op jit(solution)/shard_map/all_to_all | solution.py:186
  105.4 33.9 %all-gather.9.cloned.1.call-done = f32[16,129,128]{2,1,0:T(8,128)} async-done(((f32[1,129,128]{2,1,0:T(8,128)}), f32[16,129,128]{2,1,0:T(8,128)}) %all-gather.9.cloned.1.call-update) | async-done | bytes 1056784 | tf_op jit(solution)/shard_map/all_gather | solution.py:26
  139.2 0.8 slice.250
  140.1 0.6 fusion.77
  141.3 11.4 %fusion.56 = f32[128,128]{1,0:T(8,128)S(1)} fusion(f32[16,129,128]{2,1,0:T(8,128)} %all-gather.9.cloned.1.call-done, f32[2,129,128]{2,1,0:T(8,128)S(1)} %all-gather.2, f32[]{:T(128)} %bitcast.46, f32[]{:T(128)} %bitcast.45, f32[]{:T(128)} %bitcast.44, f32[]{:T(128)} %bitcast.43, f32[]{:T(128)} %bitcast.42, f32[]{:T(128)} %bitcast.41, f32[]{:T(128)} %bitcast.40, ...), kind=kLoop, calls=%fused_computation.80 | loop fusion | flops 884736 | bytes 1245278 | tf_op jit(solution)/shard_map/mul | solution.py:136
  153.6 17.4 %all_gather.22 = bf16[256,512]{1,0:T(8,128)(2,1)} all-gather(bf16[256,128]{1,0:T(8,128)(2,1)S(1)} %fusion.49), channel_id=1, replica_groups=mesh['ep_0'=16,'ep_1'=2,'tp_0'=4,'tp_1'=4] {'tp_1'}, dimensions={1}, use_global_device_ids=true | all-gather | bytes 327680 | tf_op jit(solution)/shard_map/all_gather | solution.py:52
  171.1 2.8 %copy.55 = bf16[16,32,2,8,256]{4,3,0,2,1:T(8,128)(2,1)S(1)} copy(bf16[16,32,2,8,256]{4,3,2,1,0:T(8,128)(2,1)} %bitcast.82) | data formatting | bytes 8388608 | tf_op jit(solution)/shard_map/reshape | solution.py:186
  173.9 1.9 convolution_convert_fusion
  175.8 10.1 %all-to-all-start.3 = ((bf16[32,16,128]{2,1,0:T(8,128)(2,1)}), bf16[32,16,128]{2,1,0:T(8,128)(2,1)S(1)}, u32[]{:S(2)}, u32[]{:S(2)}) async-start(bf16[32,16,128]{2,1,0:T(8,128)(2,1)} %convolution_convert_fusion), calls=%async_computation.3 | async-start | bytes 262144 | tf_op jit(solution)/shard_map/all_to_all | solution.py:190
  186.1 13.8 %all-gather.7.cloned.1.call-done = bf16[256,2048]{1,0:T(8,128)(2,1)} async-done(((bf16[256,512]{1,0:T(8,128)(2,1)}), bf16[256,2048]{1,0:T(8,128)(2,1)}) %all-gather.7.cloned.1.call-update) | async-done | bytes 1048592 | tf_op jit(solution)/shard_map/all_gather | solution.py:52
  200.0 2.3 %convolution_convert_fusion.1 = bf16[256,128]{1,0:T(8,128)(2,1)} fusion(bf16[256,2048]{1,0:T(8,128)(2,1)} %all-gather.7.cloned.1.call-done, bf16[2048,128]{1,0:T(8,128)(2,1)S(1)} %copy-done.2), kind=kOutput, calls=%fused_computation.24 | convolution fusion | flops 134250496 | bytes 1638400 | tf_op jit(solution)/shard_map/dot_general | solution.py:150
  202.3 0.9 all-to-all-done.3
  203.2 1.3 gather_fusion.1
  204.5 1.1 fusion.19
  (81 shorter events, 4.4 us)
Async XLA Ops:
  7.2 84.7 %copy-start = (bf16[1,2048,256]{2,1,0:T(8,128)(2,1)S(1)}, bf16[1,2048,256]{2,1,0:T(8,128)(2,1)}, u32[]{:S(2)}) copy-start(bf16[1,2048,256]{2,1,0:T(8,128)(2,1)} %param.25) | copy-start | bytes 3145732
  7.2 8.5 %copy-start.1 = (bf16[256,2048]{1,0:T(8,128)(2,1)S(1)}, bf16[256,2048]{1,0:T(8,128)(2,1)}, u32[]{:S(2)}) copy-start(bf16[256,2048]{1,0:T(8,128)(2,1)} %param.21) | copy-start | bytes 3145732
  16.0 23.0 %copy-start.14 = (f32[256,1]{0,1:T(1,128)S(1)}, f32[256,1]{0,1:T(1,128)}, u32[]{:S(2)}) copy-start(f32[256,1]{0,1:T(1,128)} %param.19) | copy-start | bytes 3076
  16.0 24.6 %copy-start.5 = (bf16[256,128]{1,0:T(8,128)(2,1)S(1)}, bf16[256,128]{1,0:T(8,128)(2,1)}, u32[]{:S(2)}) copy-start(bf16[256,128]{1,0:T(8,128)(2,1)} %param.16) | copy-start | bytes 196612
  16.0 24.6 %copy-start.6 = (bf16[256,128]{1,0:T(8,128)(2,1)S(1)}, bf16[256,128]{1,0:T(8,128)(2,1)}, u32[]{:S(2)}) copy-start(bf16[256,128]{1,0:T(8,128)(2,1)} %param.15) | copy-start | bytes 196612
  23.5 32.7 %all-to-all-start = ((bf16[32,2,1024]{2,1,0:T(2,128)(2,1)}), bf16[32,2,1024]{2,1,0:T(2,128)(2,1)S(1)}, u32[]{:S(2)}, u32[]{:S(2)}) async-start(bf16[32,2,1024]{2,1,0:T(2,128)(2,1)} %reshape.666), calls=%async_computation | async-start | bytes 262144 | tf_op jit(solution)/shard_map/all_to_all | solution.py:179
  40.0 25.7 %copy-start.12 = (f32[2]{0:T(128)}, f32[2]{0:T(128)S(1)}, u32[]{:S(2)}) copy-start(f32[2]{0:T(128)S(1)} %get-tuple-element.71) | copy-start | bytes 28
  58.0 8.2 %copy-start.7 = (bf16[256,128]{1,0:T(8,128)(2,1)S(1)}, bf16[256,128]{1,0:T(8,128)(2,1)}, u32[]{:S(2)}) copy-start(bf16[256,128]{1,0:T(8,128)(2,1)} %param.17) | copy-start | bytes 196612
  58.0 13.8 %copy-start.15 = (f32[1,128]{1,0:T(1,128)S(1)}, f32[1,128]{1,0:T(1,128)}, u32[]{:S(2)}) copy-start(f32[1,128]{1,0:T(1,128)} %pad_bitcast_fusion.1) | copy-start | bytes 1540
  58.0 33.8 %all-to-all-start.1 = ((bf16[16,32,1,2048]{3,1,2,0:T(8,128)(2,1)}), bf16[16,32,1,2048]{3,1,2,0:T(8,128)(2,1)S(1)}, u32[]{:S(2)}, u32[]{:S(2)}) async-start(bf16[16,32,1,2048]{3,1,2,0:T(8,128)(2,1)} %broadcast_in_dim.33), calls=%async_computation.1 | async-start | bytes 4194304 | tf_op jit(solution)/shard_map/all_to_all | solution.py:64
  65.6 73.6 %all-gather.9.cloned.1.call-start = ((), (), s32[]{:S(2)}) async-start(), calls=%async_computation.5 | async-start | bytes 1183744 | tf_op jit(solution)/shard_map/all_gather | solution.py:26
  91.8 1.2 copy-start.16
  96.3 8.2 %copy-start.13 = (f32[2,1]{0,1:T(1,128)S(1)}, f32[2,1]{0,1:T(1,128)}, u32[]{:S(2)}) copy-start(f32[2,1]{0,1:T(1,128)} %get-tuple-element.177) | copy-start | bytes 28
  96.3 56.4 %copy-start.3 = (bf16[256,1,64]{2,0,1:T(8,128)(2,1)S(1)}, bf16[256,1,64]{2,0,1:T(8,128)(2,1)}, u32[]{:S(2)}) copy-start(bf16[256,1,64]{2,0,1:T(8,128)(2,1)} %get-tuple-element.83) | copy-start | bytes 98308
  96.3 56.4 %copy-start.4 = (f32[2,1,128,128]{3,2,1,0:T(8,128)S(1)}, f32[2,1,128,128]{3,2,1,0:T(8,128)}, u32[]{:S(2)}) copy-start(f32[2,1,128,128]{3,2,1,0:T(8,128)} %get-tuple-element.30) | copy-start | bytes 393220
  96.3 56.4 %copy-start.10 = (f32[2,128]{1,0:T(2,128)S(1)}, f32[2,128]{1,0:T(2,128)}, u32[]{:S(2)}) copy-start(f32[2,128]{1,0:T(2,128)} %get-tuple-element.106) | copy-start | bytes 3076
  96.3 56.8 %copy-start.8 = (bf16[256,128]{1,0:T(8,128)(2,1)S(1)}, bf16[256,128]{1,0:T(8,128)(2,1)}, u32[]{:S(2)}) copy-start(bf16[256,128]{1,0:T(8,128)(2,1)} %param.17) | copy-start | bytes 196612
  96.3 74.7 %all-to-all-start.2 = ((bf16[16,32,16,256]{3,2,1,0:T(8,128)(2,1)}), bf16[16,32,16,256]{3,2,1,0:T(8,128)(2,1)}, u32[]{:S(2)}, u32[]{:S(2)}) async-start(bf16[16,32,16,256]{3,2,1,0:T(8,128)(2,1)} %stack.2), calls=%async_computation.2 | async-start | bytes 8388608 | tf_op jit(solution)/shard_map/all_to_all | solution.py:186
  104.4 49.1 %copy-start.9 = (bf16[256,128]{1,0:T(8,128)(2,1)S(1)}, bf16[256,128]{1,0:T(8,128)(2,1)}, u32[]{:S(2)}) copy-start(bf16[256,128]{1,0:T(8,128)(2,1)} %param.18) | copy-start | bytes 196612
  104.5 95.5 %all-gather.7.cloned.1.call-start = ((), (), s32[]{:S(2)}) async-start(), calls=%async_computation.4 | async-start | bytes 1310720 | tf_op jit(solution)/shard_map/all_gather | solution.py:52
  171.1 2.8 %copy-start.17 = (bf16[1,4096,128]{2,1,0:T(8,128)(2,1)S(1)}, bf16[1,4096,128]{2,1,0:T(8,128)(2,1)}, u32[]{:S(2)}) copy-start(bf16[1,4096,128]{2,1,0:T(8,128)(2,1)} %param.27) | copy-start | bytes 3145732
  173.9 12.1 %copy-start.11 = (f32[256,2]{0,1:T(2,128)S(1)}, f32[256,2]{0,1:T(2,128)}, u32[]{:S(2)}) copy-start(f32[256,2]{0,1:T(2,128)} %param.24) | copy-start | bytes 6148
  173.9 26.1 %copy-start.2 = (bf16[2048,128]{1,0:T(8,128)(2,1)S(1)}, bf16[2048,128]{1,0:T(8,128)(2,1)}, u32[]{:S(2)}) copy-start(bf16[2048,128]{1,0:T(8,128)(2,1)} %param.20) | copy-start | bytes 1572868
  175.8 27.3 %all-to-all-start.3 = ((bf16[32,16,128]{2,1,0:T(8,128)(2,1)}), bf16[32,16,128]{2,1,0:T(8,128)(2,1)S(1)}, u32[]{:S(2)}, u32[]{:S(2)}) async-start(bf16[32,16,128]{2,1,0:T(8,128)(2,1)} %convolution_convert_fusion), calls=%async_computation.3 | async-start | bytes 262144 | tf_op jit(solution)/shard_map/all_to_all | solution.py:190
Sparse Core Ops, SparseCore 0:
  77.3 61.8 all-gather.8
  171.2 28.7 all-gather.6
